TPU v7x, 32 devices: a whole 2x2x4 slice. The times are simulated.
32 devices in a mesh: grp: 2 (over y), ep: 4 (over z), tp: 4 (over x, core).
Axes of the slice: x: 2, y: 2, z: 4, core: 2. Of those that a mesh axis runs over, the one named last changes fastest.
Arguments:
- query: bfloat16 [8192, 1024], P(('grp', 'ep'), 'tp'), parts along dimension 0, may hold values from -6 to 6
- forget_gate_logits: bfloat16 [8192, 1024], P(('grp', 'ep'), 'tp'), parts along dimension 0, may hold values from -8 to 8
- value: bfloat16 [8192, 1024], P(('grp', 'ep'), 'tp'), parts along dimension 0, may hold values from -6 to 6
- forget_lower_margin: float32 [2, 1024], P(None, 'tp'), may hold values from -30 to -2
- position_log_decay: float32 [8, 8192], P('tp', ('grp', 'ep')), parts along dimension 1, may hold values from -1.5 to 0
- head_norm_gain: float32 [128], replicated, may hold values from 0.1 to 1.9
- mixer_output_weight: bfloat16 [1024, 2048], P('tp'), may hold values from -0.1875 to 0.1875
- second_batch_tokens: bfloat16 [4096, 2048], P(('grp', 'ep', 'tp')), parts along dimension 0, may hold values from -60 to 60
- expert_norm_gain: float32 [2048], replicated, may hold values from 0.1 to 1.9
- routes: int32 [4096, 2], P(('grp', 'ep', 'tp')), parts along dimension 0, may hold values from 0 to 3, all different within a row; in each aligned block of 128 rows (0 to 127, 128 to 255, ...) at most 96 rows name the same one
- chosen_expert_weight: float32 [4096, 2], P(('grp', 'ep', 'tp')), parts along dimension 0, may hold values from 0.2 to 1
- gate_weight: bfloat16 [4, 2048, 2048], P('ep', None, 'tp'), may hold values from -0.3125 to 0.3125
- up_weight: bfloat16 [4, 2048, 2048], P('ep', None, 'tp'), may hold values from -0.3125 to 0.3125
- down_weight: bfloat16 [4, 2048, 2048], P('ep', 'tp'), may hold values from -0.02734375 to 0.02734375
Outputs:
- first_mixer_output: bfloat16 [8192, 2048], P(('grp', 'ep', 'tp')), parts along dimension 0
- moe_out: bfloat16 [4096, 2048], P(('grp', 'ep', 'tp')), parts along dimension 0
There are 2 independent parts, one for each index of `grp`. A program takes and returns all parts, laid end to end along the dimension named above; an argument that names none is the same for every part. Nothing has to cross between parts.
Inputs may be any that keep to these rules, and one draw needn't show every extreme that they name: `routes`: each row names 2 different experts. Among the rows of one device no expert is named by more than 96 rows, and in every draw some expert is named by exactly 96 rows of some device.
All inputs are finite; a program needn't handle non-finite values.
Results may differ from a plain program's by a relative error of at most 0.015.
Values may be sent and summed in bfloat16 or wider, within the bound.
A program may use at most 128 MiB of HBM per device.

v0:
```python
import jax
import jax.numpy as jnp
from jax import lax
from jax.sharding import PartitionSpec as P

HEAD_CHANNELS = 128
BLK = 128


NORM_EPS = 1e-06
CLAMP_LIMIT = 7.0
SIGMOID_SCALE = 1.702
PRECISE = lax.Precision.HIGHEST


def carried_in(value, axis, combine, identity, reverse):
    length, position = (lax.axis_size(axis), lax.axis_index(axis))
    everything = jax.tree.map(
        lambda part, kind: lax.all_gather(part.astype(kind), axis),
        value,
        (jnp.bfloat16, jnp.bfloat16),
    )
    start = jax.tree.map(
        lambda part, zero: jnp.broadcast_to(jnp.asarray(zero, part.dtype), part.shape),
        value,
        identity,
    )

    def turn(k, before):
        at = length - 1 - k if reverse else k
        reached = at > position if reverse else at < position
        new = combine(
            before, jax.tree.map(lambda part, own: part[at].astype(own.dtype), everything, value)
        )
        return jax.tree.map(lambda a, b: jnp.where(reached, a, b), new, before)

    return lax.fori_loop(0, length, turn, start)


def clamped_unit(gate_pre, up_pre):
    gate_pre = jnp.minimum(gate_pre, CLAMP_LIMIT)
    up_pre = jnp.clip(up_pre, -CLAMP_LIMIT, CLAMP_LIMIT)
    return (up_pre + 1.0) * gate_pre * jax.nn.sigmoid(SIGMOID_SCALE * gate_pre)


def local_recurrence(queries, ending_state, values, forget_log_rates):
    sequence_length, number_of_heads, channels = queries.shape
    nblocks = sequence_length // BLK

    def to_blocks(array):
        return array.reshape(nblocks, BLK, number_of_heads, array.shape[-1])

    query_blocks = to_blocks(queries)
    key_blocks = to_blocks(ending_state)
    value_blocks = to_blocks(values)
    cumul = jnp.cumsum(to_blocks(forget_log_rates), axis=1)
    block_last = cumul[:, -1]
    query_in = query_blocks * jnp.exp(cumul)
    key_in = key_blocks * jnp.exp(-cumul)
    key_state = key_blocks * jnp.exp(block_last[:, None] - cumul)
    lower = jnp.tril(jnp.ones((BLK, BLK), jnp.float32))
    scores = jnp.einsum("nchd,nshd->nhcs", query_in, key_in, precision=PRECISE) * lower
    inner = jnp.einsum("nhcs,nshv->nchv", scores, value_blocks, precision=PRECISE)
    increments = jnp.einsum("nshd,nshv->nhdv", key_state, value_blocks, precision=PRECISE)

    def advance(state, inputs):
        decay, increment = inputs
        return (state * decay[..., None] + increment, state)

    initial = jnp.zeros((number_of_heads, channels, values.shape[-1]), jnp.float32)
    final_state, before = lax.scan(advance, initial, (jnp.exp(block_last), increments))
    outer = jnp.einsum("nchd,nhdv->nchv", query_in, before, precision=PRECISE)
    output = (inner + outer).reshape(sequence_length, number_of_heads, values.shape[-1])
    offsets = jnp.cumsum(block_last, axis=0) - block_last
    carried_query = (query_blocks * jnp.exp(cumul + offsets[:, None])).reshape(
        sequence_length, number_of_heads, channels
    )
    total_log = jnp.sum(block_last, axis=0)
    return (output, final_state, total_log, carried_query)


def chain_combine(earlier, later):
    return (earlier[0] * later[0], earlier[1] * later[0][..., None] + later[1])


def mixer_head_states(
    query, forget_gate_logits, value, forget_lower_margin, position_log_decay, head_norm_gain
):
    sequence_length = query.shape[0]
    number_of_heads = query.shape[1] // HEAD_CHANNELS
    queries = jax.nn.silu(query.astype(jnp.float32)).reshape(
        sequence_length, number_of_heads, HEAD_CHANNELS
    ) * HEAD_CHANNELS ** (-0.5)
    values = value.astype(jnp.float32).reshape(sequence_length, number_of_heads, HEAD_CHANNELS)
    shutting = jax.nn.sigmoid(-forget_gate_logits.astype(jnp.float32))
    decay_spikes = jnp.transpose(position_log_decay)[:, :, None]
    ending_state = jnp.exp(forget_lower_margin[0])[None, :] * shutting
    forget_log_rates = (
        jnp.log1p(-ending_state).reshape(sequence_length, number_of_heads, HEAD_CHANNELS)
        + decay_spikes
    )
    ending_state = ending_state.reshape(sequence_length, number_of_heads, HEAD_CHANNELS)
    output, final_state, total_log, carried = local_recurrence(
        queries, ending_state, values, forget_log_rates
    )
    identity = (jnp.ones_like(total_log), jnp.zeros_like(final_state))
    entering = carried_in((jnp.exp(total_log), final_state), "ep", chain_combine, identity, False)[
        1
    ]
    forward = output + jnp.einsum("lhd,hdv->lhv", carried, entering, precision=PRECISE)
    ending_state = jnp.exp(forget_lower_margin[1])[None, :] * shutting
    forget_log_rates = (
        jnp.log1p(-ending_state).reshape(sequence_length, number_of_heads, HEAD_CHANNELS)
        + decay_spikes
    )
    ending_state = ending_state.reshape(sequence_length, number_of_heads, HEAD_CHANNELS)
    output, final_state, total_log, carried = local_recurrence(
        jnp.flip(queries, 0),
        jnp.flip(ending_state, 0),
        jnp.flip(values, 0),
        jnp.flip(forget_log_rates, 0),
    )
    entering = carried_in((jnp.exp(total_log), final_state), "ep", chain_combine, identity, True)[1]
    backward = jnp.flip(
        output + jnp.einsum("lhd,hdv->lhv", carried, entering, precision=PRECISE), 0
    )
    mix = forward + backward
    scaled = (
        mix * lax.rsqrt(jnp.mean(mix * mix, axis=-1, keepdims=True) + NORM_EPS) * head_norm_gain
    )
    return scaled.reshape(sequence_length, number_of_heads * HEAD_CHANNELS).astype(jnp.bfloat16)


def body(
    query,
    forget_gate_logits,
    value,
    forget_lower_margin,
    position_log_decay,
    head_norm_gain,
    mixer_output_weight,
    second_batch_tokens,
    expert_norm_gain,
    routes,
    chosen_expert_weight,
    gate_weight,
    up_weight,
    down_weight,
):
    head_outputs = mixer_head_states(
        query, forget_gate_logits, value, forget_lower_margin, position_log_decay, head_norm_gain
    )
    tokens, top_count = routes.shape
    features = second_batch_tokens.shape[1]
    n_ep = lax.axis_size("ep")
    n_tp = lax.axis_size("tp")
    capacity = (3 * tokens * top_count + 2 * n_ep - 1) // (2 * n_ep)
    tokens_f = second_batch_tokens.astype(jnp.float32)
    normed = (
        tokens_f
        * lax.rsqrt(jnp.mean(tokens_f * tokens_f, axis=-1, keepdims=True) + NORM_EPS)
        * expert_norm_gain
    ).astype(jnp.bfloat16)
    flat_routes = routes.reshape(-1)
    onehot = (flat_routes[:, None] == jnp.arange(n_ep, dtype=jnp.int32)[None, :]).astype(jnp.int32)
    ranking = jnp.cumsum(onehot, axis=0) - onehot
    slot_index = jnp.sum(ranking * onehot, axis=1)
    destination = flat_routes * capacity + slot_index
    source = (
        jnp.full((n_ep * capacity,), tokens, jnp.int32)
        .at[destination]
        .set(jnp.arange(tokens * top_count, dtype=jnp.int32) // top_count)
    )
    padded = jnp.concatenate([normed, jnp.zeros((1, features), jnp.bfloat16)], axis=0)
    send = padded[source]
    expert_block = n_ep * capacity
    copies = jnp.broadcast_to(
        send.reshape(n_ep, 1, capacity, features), (n_ep, n_tp, capacity, features)
    ).reshape(n_ep * n_tp * capacity, features)
    arrived = lax.all_to_all(copies, ("ep", "tp"), split_axis=0, concat_axis=0, tiled=True)
    gate_pre = jnp.dot(arrived, gate_weight[0], preferred_element_type=jnp.float32)
    up_pre = jnp.dot(arrived, up_weight[0], preferred_element_type=jnp.float32)
    hidden = clamped_unit(gate_pre, up_pre).astype(jnp.bfloat16)
    picked = head_outputs
    first_mixer_output = lax.psum_scatter(
        jnp.dot(picked, mixer_output_weight, preferred_element_type=jnp.float32).astype(
            jnp.bfloat16
        ),
        "tp",
        scatter_dimension=0,
        tiled=True,
    )
    block_count = expert_block * lax.axis_size("tp") // expert_block
    grid_view = hidden.reshape(n_ep, n_tp, capacity, hidden.shape[-1])
    picked = grid_view
    picked = jnp.moveaxis(picked, 1, 0).reshape(block_count * expert_block, hidden.shape[-1])
    expert_sum = lax.psum_scatter(
        jnp.dot(picked, down_weight[0], preferred_element_type=jnp.float32).astype(jnp.bfloat16),
        "tp",
        scatter_dimension=0,
        tiled=True,
    )
    returned = lax.all_to_all(expert_sum, "ep", split_axis=0, concat_axis=0, tiled=True)
    gathered = returned[destination].reshape(tokens, top_count, features)
    moe_out = jnp.sum(
        chosen_expert_weight[:, :, None] * gathered.astype(jnp.float32), axis=1
    ).astype(jnp.bfloat16)
    return (first_mixer_output, moe_out)


def solution(mesh):
    return jax.shard_map(
        body,
        mesh=mesh,
        in_specs=(
            P(("grp", "ep"), "tp"),
            P(("grp", "ep"), "tp"),
            P(("grp", "ep"), "tp"),
            P(None, "tp"),
            P("tp", ("grp", "ep")),
            P(),
            P("tp", None),
            P(("grp", "ep", "tp"), None),
            P(),
            P(("grp", "ep", "tp"), None),
            P(("grp", "ep", "tp"), None),
            P("ep", None, "tp"),
            P("ep", None, "tp"),
            P("ep", "tp", None),
        ),
        out_specs=(P(("grp", "ep", "tp"), None), P(("grp", "ep", "tp"), None)),
        check_vma=False,
    )
```

profile of v0, /device:TPU:0, one launch (start us, length us, event | category | flops | bytes accessed | tf_op | source)
XLA Modules:
  0.0 379.9 jit_solution(997884726654975377)
XLA Ops:
  9.1 1.2 reduce-window.6
  11.0 1.4 scatter_custom_fusion
  12.4 1.2 fusion.17
  13.7 1.2 fusion.19
  15.0 3.1 gather_fusion
  18.0 4.9 %broadcast_in_dim.32 = bf16[4,4,96,2048]{3,2,1,0:T(8,128)(2,1)} broadcast(bf16[4,96,2048]{2,1,0:T(8,128)(2,1)} %bitcast.183), dimensions={0,2,3} | broadcast | bytes 7864320 | tf_op jit(solution)/shard_map/broadcast_in_dim | solution.py:177
  22.9 7.6 %all-to-all-start = ((bf16[16,96,2048]{2,1,0:T(8,128)(2,1)}), bf16[16,96,2048]{2,1,0:T(8,128)(2,1)}, u32[]{:S(2)}, u32[]{:S(2)}) async-start(bf16[16,96,2048]{2,1,0:T(8,128)(2,1)} %bitcast.178), calls=%async_computation.1 | async-start | bytes 12582912 | tf_op jit(solution)/shard_map/all_to_all | solution.py:180
  31.3 2.3 log-plus-one_bitcast_fusion
  33.9 1.4 copy.121
  35.4 1.6 fusion.31
  37.0 2.8 copy.175
  39.9 2.5 copy.123
  42.4 2.0 copy.118
  44.4 2.4 multiply_bitcast_fusion
  46.9 1.2 copy.172
  48.0 2.6 copy.122
  50.6 2.0 reshape_reshape.7
  52.7 3.4 exponential_multiply_fusion.2
  56.1 2.4 convolution_multiply_fusion.1
  58.5 1.6 convolution_bitcast_fusion.5
  60.1 2.0 fusion.25
  63.3 13.8 %while.56 = (s32[]{:T(128)}, f32[2,128,128]{2,1,0:T(8,128)S(1)}, f32[8,2,128,128]{3,2,1,0:T(8,128)}, f32[8,2,128]{2,0,1:T(8,128)S(1)}, f32[8,2,128,128]{3,2,1,0:T(8,128)}, /*index=5*/s32[]{:T(128)}, s32[]{:T(128)}) while((s32[]{:T(128)}, f32[2,128,128]{2,1,0:T(8,128)S(1)}, f32[8,2,128,128]{3,2,1,0:T(8,128)}, ...), condition=%wide.region_2.3_spmd.clone, body=%wide.region_1.2_spmd.clone.sunk | while | flops 131075 | bytes 659040 | solution.py:71
  77.1 67.4 %all-to-all-done = bf16[16,96,2048]{2,1,0:T(8,128)(2,1)} async-done(((bf16[16,96,2048]{2,1,0:T(8,128)(2,1)}), bf16[16,96,2048]{2,1,0:T(8,128)(2,1)}, u32[]{:S(2)}, u32[]{:S(2)}) %all-to-all-start) | async-done | bytes 6291488 | tf_op jit(solution)/shard_map/all_to_all | solution.py:180
  144.6 6.3 %convolution_minimum_fusion = f32[1536,512]{1,0:T(8,128)S(1)} fusion(bf16[1536,2048]{1,0:T(8,128)(2,1)} %bitcast.35, bf16[1,2048,512]{2,1,0:T(8,128)(2,1)} %param.33), kind=kOutput, calls=%fused_computation.18 | convolution fusion | flops 3222011904 | bytes 11534336 | tf_op jit(solution)/shard_map/dot_general | solution.py:181
  150.9 6.9 %fusion.5 = bf16[1536,512]{1,0:T(8,128)(2,1)S(1)} fusion(f32[1536,512]{1,0:T(8,128)S(1)} %convolution_minimum_fusion, bf16[1536,2048]{1,0:T(8,128)(2,1)} %bitcast.35, bf16[1,2048,512]{2,1,0:T(8,128)(2,1)S(1)} %copy-done.22), kind=kOutput, calls=%fused_computation.22 | convolution fusion | flops 3228303360 | bytes 13107200 | tf_op jit(solution)/shard_map/dot_general | solution.py:182
  157.9 5.4 %convolution_convert_fusion = bf16[1536,2048]{1,0:T(8,128)(2,1)} fusion(bf16[1536,512]{1,0:T(8,128)(2,1)S(1)} %bitcast.199, bf16[1,512,2048]{2,1,0:T(8,128)(2,1)S(1)} %copy-done), kind=kOutput, calls=%fused_computation.15 | convolution fusion | flops 3224371200 | bytes 9961472 | tf_op jit(solution)/shard_map/dot_general | solution.py:198
  164.9 2.1 fusion.13
  167.0 1.3 copy.146
  168.4 1.3 copy.132
  169.7 1.3 copy.137
  171.2 1.7 rev.17
  172.9 1.3 copy.139
  174.2 1.9 fusion.23
  177.1 7.5 %rev.18 = f32[1024,2,128]{0,2,1:T(8,128)S(1)} reverse(f32[1024,2,128]{0,2,1:T(8,128)} %bitcast.193), dimensions={0} | reverse | bytes 2097152 | tf_op jit(solution)/shard_map/jit(_flip)/rev | solution.py:119
  184.6 1.4 copy.142
  186.0 1.5 reverse.3
  187.6 1.3 copy.138
  188.9 5.9 %rev.19 = f32[1024,2,128]{0,2,1:T(8,128)} reverse(bf16[1024,2,128]{0,2,1:T(8,128)(2,1)S(1)} %bitcast.196), dimensions={0} | reverse | bytes 1572864 | tf_op jit(solution)/shard_map/jit(_flip)/rev | solution.py:120
  194.8 1.9 copy.147
  198.2 4.5 %exponential_multiply_fusion = (f32[8,128,2,128]{3,0,1,2:T(8,128)S(1)}, f32[8,128,2,128]{3,0,1,2:T(8,128)S(1)}, f32[8,128,2,128]{3,0,1,2:T(8,128)}, f32[8,128,2,128]{3,0,1,2:T(8,128)S(1)}) fusion(f32[8,128,2,128]{3,0,1,2:T(8,128)} %copy-done.8, f32[8,128,2,128]{3,1,0,2:T(8,128)} %bitcast.184, f32[8,2,128]{2,0,1:T(8,128)S(1)} %get-tuple-element.453, ...), kind=kLoop, calls=%fused_computation.63 | loop fusion | flops 1572864 | bytes 7356416 | tf_op jit(solution)/shard_map/mul | solution.py:60
  202.7 2.4 convolution_multiply_fusion
  205.2 2.2 convolution_bitcast_fusion.2
  207.4 2.9 fusion.20
  211.4 13.7 %while.58 = (s32[]{:T(128)}, f32[2,128,128]{2,1,0:T(8,128)S(1)}, f32[8,2,128,128]{3,2,1,0:T(8,128)}, f32[8,2,128]{2,0,1:T(8,128)S(1)}, f32[8,2,128,128]{3,2,1,0:T(8,128)}, /*index=5*/s32[]{:T(128)}, s32[]{:T(128)}) while((s32[]{:T(128)}, f32[2,128,128]{2,1,0:T(8,128)S(1)}, f32[8,2,128,128]{3,2,1,0:T(8,128)}, ...), condition=%wide.region_9.10_spmd.clone, body=%wide.region_8.9_spmd.clone.sunk | while | flops 131075 | bytes 659040 | solution.py:71
  225.0 3.4 fusion.10
  228.5 1.7 copy.154
  230.2 1.2 reshape.222
  231.4 1.2 copy.155
  232.6 2.5 copy.156
  235.1 31.4 %all-gather.5 = bf16[4,2,128]{2,1,0:T(2,128)(2,1)S(1)} all-gather(bf16[1,2,128]{2,1,0:T(2,128)(2,1)S(1)} %fusion.50), channel_id=4, replica_groups=mesh['grp'=2,'ep'=4,'tp'=4] {'ep'}, dimensions={0}, use_global_device_ids=true | all-gather | bytes 2560 | tf_op jit(solution)/shard_map/all_gather | solution.py:19
  266.6 13.9 %all-gather.3 = bf16[8,128,128]{2,1,0:T(8,128)(2,1)S(1)} all-gather(bf16[2,128,128]{2,1,0:T(8,128)(2,1)S(1)} %convert_element_type.137), channel_id=5, replica_groups=mesh['grp'=2,'ep'=4,'tp'=4] {'ep'}, dimensions={0}, use_global_device_ids=true | all-gather | bytes 327680 | tf_op jit(solution)/shard_map/all_gather | solution.py:19
  281.4 3.6 fusion.9
  285.1 9.4 %rev.20 = f32[1024,2,128]{0,2,1:T(8,128)} reverse(f32[1024,2,128]{0,2,1:T(8,128)} %fusion.9), dimensions={0} | reverse | bytes 2097152 | tf_op jit(solution)/shard_map/jit(_flip)/rev | solution.py:124
  294.5 1.2 copy.133
  295.6 2.7 copy.134
  298.4 9.7 %all-gather.4 = bf16[4,2,128]{2,1,0:T(2,128)(2,1)S(1)} all-gather(bf16[1,2,128]{2,1,0:T(2,128)(2,1)S(1)} %fusion.49), channel_id=2, replica_groups=mesh['grp'=2,'ep'=4,'tp'=4] {'ep'}, dimensions={0}, use_global_device_ids=true | all-gather | bytes 2560 | tf_op jit(solution)/shard_map/all_gather | solution.py:19
  308.1 13.8 %all-gather.1 = bf16[8,128,128]{2,1,0:T(8,128)(2,1)S(1)} all-gather(bf16[2,128,128]{2,1,0:T(8,128)(2,1)S(1)} %convert_element_type.134), channel_id=3, replica_groups=mesh['grp'=2,'ep'=4,'tp'=4] {'ep'}, dimensions={0}, use_global_device_ids=true | all-gather | bytes 327680 | tf_op jit(solution)/shard_map/all_gather | solution.py:19
  322.6 2.8 multiply_reduce_fusion.1
  325.6 3.3 convolution_convert_fusion.1
  328.9 4.4 %all-to-all-start.1 = ((bf16[4,96,2048]{2,1,0:T(8,128)(2,1)}), bf16[4,96,2048]{2,1,0:T(8,128)(2,1)}, u32[]{:S(2)}, u32[]{:S(2)}) async-start(bf16[4,96,2048]{2,1,0:T(8,128)(2,1)} %bitcast.197), calls=%async_computation.3 | async-start | bytes 3145728 | tf_op jit(solution)/shard_map/all_to_all | solution.py:203
  333.4 27.2 %all-to-all-done.1 = bf16[4,96,2048]{2,1,0:T(8,128)(2,1)} async-done(((bf16[4,96,2048]{2,1,0:T(8,128)(2,1)}), bf16[4,96,2048]{2,1,0:T(8,128)(2,1)}, u32[]{:S(2)}, u32[]{:S(2)}) %all-to-all-start.1) | async-done | bytes 1572896 | tf_op jit(solution)/shard_map/all_to_all | solution.py:203
  360.7 4.2 %gather_fusion.1 = bf16[256,2048]{1,0:T(8,128)(2,1)S(1)} fusion(bf16[384,2048]{1,0:T(8,128)(2,1)} %bitcast.43, s32[1024]{0:T(1024)S(1)} %pad_clamp_fusion), kind=kCustom, calls=%fused_computation.1 | custom fusion | bytes 2098176 | tf_op jit(solution)/shard_map/gather | solution.py:204
  364.8 2.4 reshape.232
  367.2 5.6 %multiply_reduce_fusion = bf16[128,2048]{1,0:T(8,128)(2,1)} fusion(f32[128,2,2048]{2,1,0:T(2,128)} %reshape.232, f32[128,2]{1,0:T(8,128)S(1)} %copy.159), kind=kLoop, calls=%fused_computation.26 | loop fusion | flops 786432 | bytes 2622464 | tf_op jit(solution)/shard_map/reduce_sum | solution.py:205
  (169 shorter events, 40.4 us)
Async XLA Ops:
  7.2 150.8 %copy-start = (bf16[1,512,2048]{2,1,0:T(8,128)(2,1)S(1)}, bf16[1,512,2048]{2,1,0:T(8,128)(2,1)}, u32[]{:S(2)}) copy-start(bf16[1,512,2048]{2,1,0:T(8,128)(2,1)} %param.35) | copy-start | bytes 6291460
  22.9 8.2 %copy-start.17 = (bf16[1024,256]{1,0:T(8,128)(2,1)S(1)}, bf16[1024,256]{1,0:T(8,128)(2,1)}, u32[]{:S(2)}) copy-start(bf16[1024,256]{1,0:T(8,128)(2,1)} %param.23) | copy-start | bytes 1572868
  22.9 8.4 %copy-start.19 = (f32[2,256]{1,0:T(2,128)S(1)}, f32[2,256]{1,0:T(2,128)}, u32[]{:S(2)}) copy-start(f32[2,256]{1,0:T(2,128)} %param.25) | copy-start | bytes 6148
  22.9 121.6 %all-to-all-start = ((bf16[16,96,2048]{2,1,0:T(8,128)(2,1)}), bf16[16,96,2048]{2,1,0:T(8,128)(2,1)}, u32[]{:S(2)}, u32[]{:S(2)}) async-start(bf16[16,96,2048]{2,1,0:T(8,128)(2,1)} %bitcast.178), calls=%async_computation.1 | async-start | bytes 12582912 | tf_op jit(solution)/shard_map/all_to_all | solution.py:180
  30.5 298.4 %reduce-scatter.5.cloned.1.call-start = ((), (), s32[]{:S(2)}) async-start(), calls=%async_computation.5 | async-start | bytes 7864320 | tf_op jit(solution)/shard_map/reduce_scatter | solution.py:197
  33.7 1.6 copy-start.18
  37.0 15.7 %copy-start.7 = (f32[8,128,2,128]{3,0,1,2:T(8,128)}, f32[8,128,2,128]{3,0,1,2:T(8,128)S(1)}, u32[]{:S(2)}) copy-start(f32[8,128,2,128]{3,0,1,2:T(8,128)S(1)} %fusion.31) | copy-start | bytes 3145732
  56.1 2.4 copy-start.6
  144.6 6.3 %copy-start.22 = (bf16[1,2048,512]{2,1,0:T(8,128)(2,1)S(1)}, bf16[1,2048,512]{2,1,0:T(8,128)(2,1)}, u32[]{:S(2)}) copy-start(bf16[1,2048,512]{2,1,0:T(8,128)(2,1)} %param.34) | copy-start | bytes 6291460
  163.3 1.2 copy-start.14
  163.3 1.5 copy-start.15
  163.3 209.5 %reduce-scatter.3.cloned.1.call-start = ((), (), s32[]{:S(2)}) async-start(), calls=%async_computation.4 | async-start | bytes 5242880 | tf_op jit(solution)/shard_map/reduce_scatter | solution.py:185
  167.0 4.0 %copy-start.13 = (f32[1024,256]{0,1:T(8,128)S(1)}, f32[1024,256]{0,1:T(8,128)}, u32[]{:S(2)}) copy-start(f32[1024,256]{0,1:T(8,128)} %get-tuple-element.462) | copy-start | bytes 3145732
  174.2 11.8 %copy-start.2 = (f32[1024,256]{0,1:T(8,128)S(1)}, f32[1024,256]{0,1:T(8,128)}, u32[]{:S(2)}) copy-start(f32[1024,256]{0,1:T(8,128)} %get-tuple-element.461) | copy-start | bytes 3145732
  176.1 1.0 copy-start.8
  187.5 9.3 %copy-start.4 = (f32[1024,2,128]{0,2,1:T(8,128)}, f32[1024,2,128]{0,2,1:T(8,128)S(1)}, u32[]{:S(2)}) copy-start(f32[1024,2,128]{0,2,1:T(8,128)S(1)} %reverse.3) | copy-start | bytes 3145732
  210.3 14.8 %copy-start.11 = (f32[8,128,2,128]{3,1,2,0:T(8,128)S(1)}, f32[8,128,2,128]{3,1,2,0:T(8,128)}, u32[]{:S(2)}) copy-start(f32[8,128,2,128]{3,1,2,0:T(8,128)} %convolution_bitcast_fusion.2) | copy-start | bytes 3145732
  228.5 2.9 copy-start.10
  231.4 50.0 %copy-start.5 = (f32[1024,2,128]{0,2,1:T(8,128)S(1)}, f32[1024,2,128]{0,2,1:T(8,128)}, u32[]{:S(2)}) copy-start(f32[1024,2,128]{0,2,1:T(8,128)} %copy-done.4) | copy-start | bytes 3145732
  281.4 13.0 %copy-start.9 = (f32[8,128,2,128]{3,0,1,2:T(8,128)S(1)}, f32[8,128,2,128]{3,0,1,2:T(8,128)}, u32[]{:S(2)}) copy-start(f32[8,128,2,128]{3,0,1,2:T(8,128)} %get-tuple-element.446) | copy-start | bytes 3145732
  294.5 28.1 %copy-start.3 = (f32[1024,256]{0,1:T(8,128)S(1)}, f32[1024,256]{0,1:T(8,128)}, u32[]{:S(2)}) copy-start(f32[1024,256]{0,1:T(8,128)} %get-tuple-element.461) | copy-start | bytes 3145732
  295.6 26.9 %copy-start.12 = (f32[1024,2,128]{0,2,1:T(8,128)S(1)}, f32[1024,2,128]{0,2,1:T(8,128)}, u32[]{:S(2)}) copy-start(f32[1024,2,128]{0,2,1:T(8,128)} %copy.137) | copy-start | bytes 3145732
  322.6 2.8 copy-start.21
  322.6 3.0 copy-start.16
  328.9 4.4 %copy-start.20 = (f32[128,2]{0,1:T(2,128)S(1)}, f32[128,2]{0,1:T(2,128)}, u32[]{:S(2)}) copy-start(f32[128,2]{0,1:T(2,128)} %param.32) | copy-start | bytes 3076
  328.9 31.7 %all-to-all-start.1 = ((bf16[4,96,2048]{2,1,0:T(8,128)(2,1)}), bf16[4,96,2048]{2,1,0:T(8,128)(2,1)}, u32[]{:S(2)}, u32[]{:S(2)}) async-start(bf16[4,96,2048]{2,1,0:T(8,128)(2,1)} %bitcast.197), calls=%async_computation.3 | async-start | bytes 3145728 | tf_op jit(solution)/shard_map/all_to_all | solution.py:203
  360.7 12.1 %copy-start.1 = (bf16[1,512,2048]{2,1,0:T(8,128)(2,1)S(1)}, bf16[1,512,2048]{2,1,0:T(8,128)(2,1)}, u32[]{:S(2)}) copy-start(bf16[1,512,2048]{2,1,0:T(8,128)(2,1)} %param.35) | copy-start | bytes 6291460
Sparse Core Ops, SparseCore 0:
  163.5 81.5 reduce-scatter.4
  329.0 43.6 reduce-scatter.2
where the time goes:
time: 386 us; the launch traced here: 380 us
  waiting for transfers between devices  94.7 us (25%)
  local copies, waits for them, and re-layouts  84.9 us (22%)
  blocking collectives  68.8 us (18%)
  other arithmetic  55.6 us (14%)
  matrix products  47.5 us (12%)
  between operations  14.8 us (4%)
  starting transfers between devices  12.5 us (3%)
    all_gather x4, blocking collectives, carried_in(): lax.all_gather(part.astype(kind), axis)  68.8 us
    all_to_all x1, waiting for transfers between devices, body(): lax.all_to_all(copies, ('ep', 'tp'), split_axis=0, concat_axis=0, tiled=T...  67.4 us
    all_to_all x1, waiting for transfers between devices, body(): lax.all_to_all(expert_sum, 'ep', split_axis=0, concat_axis=0, tiled=True)  27.2 us
    add x16, other arithmetic, advance(): return (state * decay[..., None] + increment, state)  16.3 us
    unnamed x55, local copies, waits for them, and re-layouts  11.4 us
    dynamic_update_slice x16, other arithmetic, local_recurrence(): lax.scan(advance, initial, (jnp.exp(block_last), increments))  10.6 us
    rev x1, local copies, waits for them, and re-layouts, mixer_head_states(): jnp.flip(output + jnp.einsum('lhd,hdv->lhv', carried, entering, precision...  9.37 us
    rev x2, local copies, waits for them, and re-layouts, mixer_head_states(): jnp.flip(ending_state, 0)  8.89 us
  transfers between devices with their start and end apart: 4, of which 2 were waited for; matrix products, arithmetic and copies ran while one was open for 40% of the time, Pallas kernels for 0%

commit v1 on v0

v1 whole, which is shorter than its diff:
```python
import functools

import jax
import jax.numpy as jnp
from jax import lax
from jax.experimental import pallas as pl
from jax.experimental.pallas import tpu as pltpu
from jax.sharding import PartitionSpec as P

HEAD_CHANNELS = 128
BLK = 128
NORM_EPS = 1e-06
CLAMP_LIMIT = 7.0
SIGMOID_SCALE = 1.702
MESH = pl.DeviceIdType.MESH
F32, BF16 = jnp.float32, jnp.bfloat16
VMEM = pl.BlockSpec(memory_space=pltpu.VMEM)
ANY = pl.BlockSpec(memory_space=pl.ANY)


def clamped_unit(gate_pre, up_pre):
    gate_pre = jnp.minimum(gate_pre, CLAMP_LIMIT)
    up_pre = jnp.clip(up_pre, -CLAMP_LIMIT, CLAMP_LIMIT)
    return (up_pre + 1.0) * gate_pre * jax.nn.sigmoid(SIGMOID_SCALE * gate_pre)


def dot(a, b, ca=1, cb=0):
    return lax.dot_general(a, b, (((ca,), (cb,)), ((), ())), preferred_element_type=F32)


def mixer_kernel(
    n_ep, q_ref, g_ref, v_ref, m_ref, pos_ref, gain_ref, w_ref, o_ref,
    q_in, inner, inc, dec, snd, got, send_sem, recv_sem,
):
    tokens, width = q_ref.shape
    heads, nblk = width // HEAD_CHANNELS, tokens // BLK
    me = lax.axis_index("ep")
    barrier = pltpu.get_barrier_semaphore()
    for k in range(1, n_ep):
        pl.semaphore_signal(
            barrier, inc=1, device_id={"ep": lax.rem(me + k, n_ep)}, device_id_type=MESH
        )

    row = lax.broadcasted_iota(jnp.int32, (BLK, BLK), 0)
    col = lax.broadcasted_iota(jnp.int32, (BLK, BLK), 1)
    masks = (row >= col, row <= col)
    floor = jnp.exp(m_ref[...])

    def cols(h):
        return slice(h * HEAD_CHANNELS, (h + 1) * HEAD_CHANNELS)

    def block_rows(b):
        return pl.ds(pl.multiple_of(b * BLK, BLK), BLK)

    def local(b, carry):
        rows = block_rows(b)
        q = q_ref[rows, :].astype(F32)
        q = q * jax.nn.sigmoid(q) * HEAD_CHANNELS ** (-0.5)
        shut = jax.nn.sigmoid(-g_ref[rows, :].astype(F32))
        v = v_ref[rows, :]
        pos_rows = pos_ref[rows, :]
        pos = jnp.concatenate(
            [jnp.broadcast_to(pos_rows[:, h : h + 1], (BLK, HEAD_CHANNELS)) for h in range(heads)],
            axis=1,
        )
        scores = [None] * heads
        for d in range(2):
            key = floor[d : d + 1, :] * shut
            rate = jnp.log1p(-key) + pos
            hi = rate.astype(BF16)
            lo = (rate - hi.astype(F32)).astype(BF16)
            tri = masks[d].astype(F32).astype(BF16)
            cumul = dot(tri, hi) + dot(tri, lo)
            last = cumul[BLK - 1 :, :] if d == 0 else cumul[:1, :]
            query_in = (q * jnp.exp(cumul)).astype(BF16)
            key_in = (key * jnp.exp(-cumul)).astype(BF16)
            key_state = (key * jnp.exp(last - cumul)).astype(BF16)
            q_in[d, rows, :] = query_in
            dec[b, d : d + 1, :] = jnp.exp(last)
            for h in range(heads):
                s = dot(query_in[:, cols(h)], key_in[:, cols(h)], 1, 1)
                s = jnp.where(masks[d], s, 0.0)
                scores[h] = s if d == 0 else scores[h] + s
                inc[d, b, :, cols(h)] = dot(v[:, cols(h)], key_state[:, cols(h)], 0, 0)
        for h in range(heads):
            inner[rows, cols(h)] = dot(scores[h].astype(BF16), v[:, cols(h)])
        return carry

    lax.fori_loop(0, nblk, local, 0)

    for d in range(2):
        def advance(i, carry, d=d):
            state, total = carry
            b = i if d == 0 else nblk - 1 - i
            decay = dec[b, d : d + 1, :]
            return state * decay + inc[d, b], total * decay

        state, total = lax.fori_loop(
            0, nblk, advance, (jnp.zeros((HEAD_CHANNELS, width), F32), jnp.ones((1, width), F32))
        )
        snd[d, :HEAD_CHANNELS, :] = state.astype(BF16)
        snd[d, HEAD_CHANNELS:, :] = jnp.broadcast_to(total, (16, width)).astype(BF16)

    pl.semaphore_wait(barrier, n_ep - 1)
    copies = []
    for k in range(1, n_ep):
        copy = pltpu.make_async_remote_copy(
            src_ref=snd,
            dst_ref=got.at[k],
            send_sem=send_sem.at[k],
            recv_sem=recv_sem.at[k],
            device_id={"ep": lax.rem(me + k, n_ep)},
            device_id_type=MESH,
        )
        copy.start()
        copies.append(copy)
    for copy in copies:
        copy.wait()

    entering = []
    for d in range(2):
        state = jnp.zeros((HEAD_CHANNELS, width), F32)
        for k in range(n_ep - 1, 0, -1):
            slot = k if d == 0 else n_ep - k
            valid = (me - k >= 0) if d == 0 else (me + k < n_ep)
            decay = got[slot, d, HEAD_CHANNELS:, :].astype(F32)[:1, :]
            new = state * decay + got[slot, d, :HEAD_CHANNELS, :].astype(F32)
            state = jnp.where(valid, new, state)
        entering.append(state)

    def ahead(b, state):
        rows = block_rows(b)
        low = state.astype(BF16)
        for h in range(heads):
            inner[rows, cols(h)] += dot(q_in[0, rows, cols(h)], low[:, cols(h)], 1, 1)
        return state * dec[b, 0:1, :] + inc[0, b]

    lax.fori_loop(0, nblk, ahead, entering[0])
    gain = gain_ref[...]

    def back(i, state):
        b = nblk - 1 - i
        rows = block_rows(b)
        low = state.astype(BF16)
        outs = []
        for h in range(heads):
            mix = inner[rows, cols(h)] + dot(q_in[1, rows, cols(h)], low[:, cols(h)], 1, 1)
            mean = jnp.mean(mix * mix, axis=-1, keepdims=True)
            outs.append((mix * lax.rsqrt(mean + NORM_EPS) * gain).astype(BF16))
        o_ref[rows, :] = dot(jnp.concatenate(outs, axis=1), w_ref[...]).astype(BF16)
        return state * dec[b, 1:2, :] + inc[1, b]

    lax.fori_loop(0, nblk, back, entering[1])


def mixer(n_ep, query, logits, value, margin, pos, gain, weight):
    tokens, width = query.shape
    features = weight.shape[1]
    nblk = tokens // BLK
    return pl.pallas_call(
        functools.partial(mixer_kernel, n_ep),
        out_shape=jax.ShapeDtypeStruct((tokens, features), BF16),
        in_specs=[VMEM] * 7,
        out_specs=VMEM,
        scratch_shapes=[
            pltpu.VMEM((2, tokens, width), BF16),
            pltpu.VMEM((tokens, width), F32),
            pltpu.VMEM((2, nblk, HEAD_CHANNELS, width), F32),
            pltpu.VMEM((nblk, 2, width), F32),
            pltpu.VMEM((2, HEAD_CHANNELS + 16, width), BF16),
            pltpu.VMEM((n_ep, 2, HEAD_CHANNELS + 16, width), BF16),
            pltpu.SemaphoreType.DMA((n_ep,)),
            pltpu.SemaphoreType.DMA((n_ep,)),
        ],
        compiler_params=pltpu.CompilerParams(
            collective_id=0, has_side_effects=True, vmem_limit_bytes=28 << 20
        ),
        cost_estimate=pl.CostEstimate(
            flops=20_000_000_000, bytes_accessed=8_000_000, transcendentals=0
        ),
        name="mixer",
    )(query, logits, value, margin, pos, gain, weight)


def expert_kernel(
    chunks, x_hbm, g_hbm, u_hbm, d_hbm, o_ref,
    x, wg, wu, wd, xc, xp, own, mid, to_c, from_c, to_d, from_d, to_p, from_p,
    load_sem, core_send, core_recv, link_send, link_recv,
):
    rows, features = x.shape
    n = rows // chunks
    t = lax.axis_index("tp")
    core = t + 1 - 2 * lax.rem(t, 2)
    peer = lax.rem(t + 2, 4)

    loads = [
        pltpu.make_async_copy(s, d, load_sem.at[i])
        for i, (s, d) in enumerate(((x_hbm, x), (g_hbm, wg), (u_hbm, wu), (d_hbm, wd)))
    ]
    for load in loads:
        load.start()
    barrier = pltpu.get_barrier_semaphore()
    for other in (core, peer):
        pl.semaphore_signal(barrier, inc=1, device_id={"tp": other}, device_id_type=MESH)
    pl.semaphore_wait(barrier, 2)

    def remote(src, dst, sends, recvs, index, other):
        return pltpu.make_async_remote_copy(
            src_ref=src,
            dst_ref=dst,
            send_sem=sends.at[index],
            recv_sem=recvs.at[index],
            device_id={"tp": other},
            device_id_type=MESH,
        )

    def mlp(block, store):
        hidden = clamped_unit(dot(block, wg[...]), dot(block, wu[...])).astype(BF16)
        step = 512 if features % 512 == 0 else features
        for at in range(0, features, step):
            store(slice(at, at + step), dot(hidden, wd[:, at : at + step]))

    def part(i):
        return pl.ds(i * n, n)

    loads[0].wait()
    gather = [
        remote(x.at[part(i)], xp.at[i, 0], link_send, link_recv, i, peer) for i in range(chunks)
    ]
    for copy in gather:
        copy.start()
    across = remote(x, xc, core_send, core_recv, 0, core)
    across.start()
    for load in loads[1:]:
        load.wait()

    def keep_own(at, value):
        own[:, at] = value

    mlp(x[...], keep_own)
    across.wait()

    def keep_core(at, value):
        to_c[:, at] = value.astype(BF16)

    mlp(xc[...], keep_core)
    give = remote(to_c, from_c, core_send, core_recv, 1, core)
    give.start()

    later = []
    for i in range(chunks):
        gather[i].wait_recv()
        forward = remote(xp.at[i, 0], xp.at[i, 1], core_send, core_recv, 2 + i, core)
        forward.start()
        forward.wait_recv()

        def keep_pair(at, value, i=i):
            mid[:, at] = value[:n]
            to_d[i, :, at] = value[n:].astype(BF16)

        mlp(xp[i].reshape(2 * n, features), keep_pair)
        swap = remote(to_d.at[i], from_d.at[i], core_send, core_recv, 2 + chunks + i, core)
        swap.start()
        swap.wait_recv()
        to_p[i] = (mid[...] + from_d[i].astype(F32)).astype(BF16)
        back = remote(to_p.at[i], from_p.at[i], link_send, link_recv, chunks + i, peer)
        back.start()
        later.append((forward, swap, back))

    give.wait_recv()
    for i in range(chunks):
        later[i][2].wait_recv()
        o_ref[part(i), :] = (
            own[part(i), :] + from_c[part(i), :].astype(F32) + from_p[i].astype(F32)
        ).astype(BF16)
    give.wait_send()
    for i in range(chunks):
        gather[i].wait_send()
        for copy in later[i]:
            copy.wait_send()


def experts(x, gate_weight, up_weight, down_weight):
    rows, features = x.shape
    hidden = gate_weight.shape[1]
    chunks = next(k for k in (3, 4, 2, 1) if rows % (16 * k) == 0 or k == 1)
    n = rows // chunks
    return pl.pallas_call(
        functools.partial(expert_kernel, chunks),
        out_shape=jax.ShapeDtypeStruct((rows, features), BF16),
        in_specs=[ANY] * 4,
        out_specs=VMEM,
        scratch_shapes=[
            pltpu.VMEM((rows, features), BF16),
            pltpu.VMEM((features, hidden), BF16),
            pltpu.VMEM((features, hidden), BF16),
            pltpu.VMEM((hidden, features), BF16),
            pltpu.VMEM((rows, features), BF16),
            pltpu.VMEM((chunks, 2, n, features), BF16),
            pltpu.VMEM((rows, features), F32),
            pltpu.VMEM((n, features), F32),
            pltpu.VMEM((rows, features), BF16),
            pltpu.VMEM((rows, features), BF16),
            pltpu.VMEM((chunks, n, features), BF16),
            pltpu.VMEM((chunks, n, features), BF16),
            pltpu.VMEM((chunks, n, features), BF16),
            pltpu.VMEM((chunks, n, features), BF16),
            pltpu.SemaphoreType.DMA((4,)),
            pltpu.SemaphoreType.DMA((2 + 2 * chunks,)),
            pltpu.SemaphoreType.DMA((2 + 2 * chunks,)),
            pltpu.SemaphoreType.DMA((2 * chunks,)),
            pltpu.SemaphoreType.DMA((2 * chunks,)),
        ],
        compiler_params=pltpu.CompilerParams(
            collective_id=1, has_side_effects=True, vmem_limit_bytes=48 << 20
        ),
        cost_estimate=pl.CostEstimate(
            flops=40_000_000_000, bytes_accessed=12_000_000, transcendentals=0
        ),
        name="experts",
    )(x, gate_weight, up_weight, down_weight)


def body(
    query,
    forget_gate_logits,
    value,
    forget_lower_margin,
    position_log_decay,
    head_norm_gain,
    mixer_output_weight,
    second_batch_tokens,
    expert_norm_gain,
    routes,
    chosen_expert_weight,
    gate_weight,
    up_weight,
    down_weight,
):
    tokens, top_count = routes.shape
    features = second_batch_tokens.shape[1]
    n_ep = lax.axis_size("ep")
    capacity = (3 * tokens * top_count + 2 * n_ep - 1) // (2 * n_ep)
    tokens_f = second_batch_tokens.astype(F32)
    normed = (
        tokens_f
        * lax.rsqrt(jnp.mean(tokens_f * tokens_f, axis=-1, keepdims=True) + NORM_EPS)
        * expert_norm_gain
    ).astype(BF16)
    named = routes[:, :, None] == jnp.arange(n_ep, dtype=jnp.int32)[None, None, :]
    chosen = jnp.any(named, axis=1)
    earlier = jnp.tril(jnp.ones((tokens, tokens), BF16), -1)
    ranking = dot(earlier, chosen.astype(BF16)).astype(jnp.int32)
    slot = jnp.where(named, ranking[:, None, :] + jnp.arange(n_ep) * capacity, 0)
    destination = jnp.sum(slot, axis=2)
    places = jnp.arange(n_ep * capacity, dtype=jnp.int32)
    hit = destination[:, :, None] == places
    pick = jnp.any(hit, axis=1).astype(BF16)
    share = jnp.sum(jnp.where(hit, chosen_expert_weight[:, :, None], 0.0), axis=1)
    share_hi = share.astype(BF16)
    share_lo = (share - share_hi.astype(F32)).astype(BF16)
    send = dot(pick, normed, 0, 0).astype(BF16)
    arrived = lax.all_to_all(send, "ep", split_axis=0, concat_axis=0, tiled=True)

    mixed = mixer(
        n_ep,
        query,
        forget_gate_logits,
        value,
        forget_lower_margin,
        jnp.transpose(position_log_decay),
        head_norm_gain[None, :],
        mixer_output_weight,
    )
    first_mixer_output = lax.psum_scatter(mixed, "tp", scatter_dimension=0, tiled=True)
    expert_sum = experts(arrived, gate_weight[0], up_weight[0], down_weight[0])
    returned = lax.all_to_all(expert_sum, "ep", split_axis=0, concat_axis=0, tiled=True)
    moe_out = (dot(share_hi, returned) + dot(share_lo, returned)).astype(BF16)
    return (first_mixer_output, moe_out)


def solution(mesh):
    return jax.shard_map(
        body,
        mesh=mesh,
        in_specs=(
            P(("grp", "ep"), "tp"),
            P(("grp", "ep"), "tp"),
            P(("grp", "ep"), "tp"),
            P(None, "tp"),
            P("tp", ("grp", "ep")),
            P(),
            P("tp", None),
            P(("grp", "ep", "tp"), None),
            P(),
            P(("grp", "ep", "tp"), None),
            P(("grp", "ep", "tp"), None),
            P("ep", None, "tp"),
            P("ep", None, "tp"),
            P("ep", "tp", None),
        ),
        out_specs=(P(("grp", "ep", "tp"), None), P(("grp", "ep", "tp"), None)),
        check_vma=False,
    )
```

time: 386 us -> 222 us (0.58); the launches traced: 380 us -> 221 us
  Pallas kernels: 0 us -> 145 us
  local copies, waits for them, and re-layouts: 84.9 us -> 6.86 us
  blocking collectives: 68.8 us -> 0 us
  waiting for transfers between devices: 94.7 us -> 36.4 us
  other arithmetic: 55.6 us -> 2.9 us
  matrix products: 47.5 us -> 4.77 us
    pallas_call x0 -> x2, Pallas kernels: none -> 145 us  [the longest x1 94.6 us: experts(): pl.pallas_call(functools.partial(expert_kernel, chunks), out_shape=jax.Sh...]
    all_gather x4 -> x0, blocking collectives: 68.8 us -> none  [carried_in(): lax.all_gather(part.astype(kind), axis)]
    all_to_all x1, waiting for transfers between devices: 67.4 us -> 0.01 us  [body(): lax.all_to_all(send, 'ep', split_axis=0, concat_axis=0, tiled=True)]
    dot_general x14 -> x4, matrix products: 47.5 us -> 4.77 us  [dot(): lax.dot_general(a, b, (((ca,), (cb,)), ((), ())), preferred_element_type=...]
    rev x8 -> x0, local copies, waits for them, and re-layouts: 30.4 us -> none  [the longest x1 9.37 us: mixer_head_states(): jnp.flip(output + jnp.einsum('lhd,hdv->lhv', carried, entering, precision...]
    add x19 -> x1, other arithmetic: 17.2 us -> 0.01 us  [body(): earlier = jnp.tril(jnp.ones((tokens, tokens), BF16), -1)]
    dynamic_update_slice x16 -> x0, other arithmetic: 10.6 us -> none  [local_recurrence(): lax.scan(advance, initial, (jnp.exp(block_last), increments))]
    all_to_all x1, waiting for transfers between devices: 27.2 us -> 36.4 us  [body(): lax.all_to_all(expert_sum, 'ep', split_axis=0, concat_axis=0, tiled=True)]
  transfers between devices with their start and end apart: 4 -> 3, of which waited for: 2 -> 1; matrix products, arithmetic and copies ran while one was open for 40% -> 1% of each run, Pallas kernels for 0% -> 65%
where the time goes in v1:
time: 222 us; the launch traced here: 221 us
  Pallas kernels  145 us (65%)
  waiting for transfers between devices  36.4 us (16%)
  between operations  14.2 us (6%)
  starting transfers between devices  11.4 us (5%)
  local copies, waits for them, and re-layouts  6.86 us (3%)
  matrix products  4.77 us (2%)
  other arithmetic  2.9 us (1%)
    pallas_call x1, Pallas kernels, experts(): pl.pallas_call(functools.partial(expert_kernel, chunks), out_shape=jax.Sh...  94.6 us
    pallas_call x1, Pallas kernels, mixer(): pl.pallas_call(functools.partial(mixer_kernel, n_ep), out_shape=jax.Shape...  49.9 us
    all_to_all x1, waiting for transfers between devices, body(): lax.all_to_all(expert_sum, 'ep', split_axis=0, concat_axis=0, tiled=True)  36.4 us
    unnamed x21, local copies, waits for them, and re-layouts  6.86 us
    all_to_all x1, starting transfers between devices, body(): lax.all_to_all(send, 'ep', split_axis=0, concat_axis=0, tiled=True)  6.49 us
    all_to_all x1, starting transfers between devices, body(): lax.all_to_all(expert_sum, 'ep', split_axis=0, concat_axis=0, tiled=True)  4.91 us
    dot_general x4, matrix products, dot(): lax.dot_general(a, b, (((ca,), (cb,)), ((), ())), preferred_element_type=...  4.77 us
  transfers between devices with their start and end apart: 3, of which 1 were waited for; matrix products, arithmetic and copies ran while one was open for 1% of the time, Pallas kernels for 65%

profile of v1, /device:TPU:0, one launch (start us, length us, event | category | flops | bytes accessed | tf_op | source)
XLA Modules:
  0.0 221.0 jit_solution(6351380058201043151)
XLA Ops:
  7.2 0.7 fusion.17
  7.9 0.2 fusion.1
  8.1 0.7 select_reduce_fusion.1
  8.8 0.1 fusion.8
  8.9 1.2 fusion.2
  10.2 2.9 %convolution_convert_fusion = bf16[384,2048]{1,0:T(8,128)(2,1)} fusion(pred[128,384]{1,0:T(8,128)(4,1)S(1)} %fusion.8, bf16[128,2048]{1,0:T(8,128)(2,1)} %param.21, f32[2048]{0:T(1024)} %param.22, f32[128]{0:T(128)S(1)} %add_rsqrt_fusion), kind=kOutput, calls=%fused_computation | convolution fusion | flops 203161600 | bytes 2155008 | tf_op jit(solution)/shard_map/dot_general | solution.py:28
  13.0 0.0 copy-start.8
  13.0 0.0 copy-start.2
  13.0 0.0 copy-start.6
  13.1 0.0 copy-start.7
  13.1 6.5 %all-to-all-start = ((bf16[4,96,2048]{2,1,0:T(8,128)(2,1)}), bf16[4,96,2048]{2,1,0:T(8,128)(2,1)S(1)}, u32[]{:S(2)}, u32[]{:S(2)}) async-start(bf16[4,96,2048]{2,1,0:T(8,128)(2,1)} %bitcast.19), calls=%async_computation.1 | async-start | bytes 3145728 | tf_op jit(solution)/shard_map/all_to_all | solution.py:363
  19.6 0.0 reduce-scatter.2.cloned.1.call-start
  19.6 0.0 copy-done.8
  19.6 0.2 copy.20
  19.8 0.0 copy-done.2
  19.8 0.0 copy-done.6
  19.8 0.0 copy-done.7
  19.8 0.0 copy-start.3
  19.8 1.0 copy-done.3
  20.9 0.0 copy-start.4
  20.9 1.0 copy-done.4
  21.9 0.0 copy-start.5
  21.9 1.0 copy-done.5
  22.9 49.9 %mixer.1 = bf16[1024,2048]{1,0:T(8,128)(2,1)S(1)} custom-call(bf16[1024,256]{1,0:T(8,128)(2,1)S(1)} %copy-done.3, bf16[1024,256]{1,0:T(8,128)(2,1)S(1)} %copy-done.4, bf16[1024,256]{1,0:T(8,128)(2,1)S(1)} %copy-done.5, f32[2,256]{1,0:T(2,128)S(1)} %copy-done.6, f32[1024,2]{1,0:T(8,128)S(1)} %bitcast.14, f32[1,128]{1,0:T(1,128)S(1)} %bitcast.16, ...), custom_call_target="tpu_custom_call" | custom-call | flops 20000000000 | bytes 8000000 | tf_op jit(solution)/shard_map/mixer/pallas_call | solution.py:160
  72.8 0.0 copy-start
  72.9 1.9 copy-done
  74.8 0.0 reduce-scatter.2.cloned.1.call-update
  74.8 0.0 all-to-all-done
  74.8 0.0 copy-start.1
  74.8 1.6 copy-done.1
  76.4 94.6 %experts.1 = bf16[384,2048]{1,0:T(8,128)(2,1)} custom-call(bf16[384,2048]{1,0:T(8,128)(2,1)S(1)} %bitcast.13, bf16[2048,512]{1,0:T(8,128)(2,1)S(1)} %bitcast.15, bf16[2048,512]{1,0:T(8,128)(2,1)} %bitcast.20, bf16[512,2048]{1,0:T(8,128)(2,1)} %bitcast.21), custom_call_target="tpu_custom_call" | custom-call | flops 40000000000 | bytes 12000000 | tf_op jit(solution)/shard_map/experts/pallas_call | solution.py:288
  171.0 0.0 copy-start.9
  171.0 4.9 %all-to-all-start.1 = ((bf16[4,96,2048]{2,1,0:T(8,128)(2,1)}), bf16[4,96,2048]{2,1,0:T(8,128)(2,1)S(1)}, u32[]{:S(2)}, u32[]{:S(2)}) async-start(bf16[4,96,2048]{2,1,0:T(8,128)(2,1)} %bitcast.7), calls=%async_computation.2 | async-start | bytes 3145728 | tf_op jit(solution)/shard_map/all_to_all | solution.py:377
  176.0 0.0 copy-done.9
  176.0 0.1 select_reduce_fusion
  176.1 36.4 %all-to-all-done.1 = bf16[4,96,2048]{2,1,0:T(8,128)(2,1)S(1)} async-done(((bf16[4,96,2048]{2,1,0:T(8,128)(2,1)}), bf16[4,96,2048]{2,1,0:T(8,128)(2,1)S(1)}, u32[]{:S(2)}, u32[]{:S(2)}) %all-to-all-start.1) | async-done | bytes 1572896 | tf_op jit(solution)/shard_map/all_to_all | solution.py:377
  212.5 0.4 fusion.11
  212.9 1.2 fusion
  214.2 0.0 reduce-scatter.2.cloned.1.call-done
  (3 shorter events, 0.0 us)
Async XLA Ops:
  13.0 6.5 %copy-start.8 = (f32[2,1024]{1,0:T(2,128)S(1)}, f32[2,1024]{1,0:T(2,128)}, u32[]{:S(2)}) copy-start(f32[2,1024]{1,0:T(2,128)} %param.18) | copy-start | bytes 24580
  13.0 6.7 %copy-start.2 = (bf16[256,2048]{1,0:T(8,128)(2,1)S(1)}, bf16[256,2048]{1,0:T(8,128)(2,1)}, u32[]{:S(2)}) copy-start(bf16[256,2048]{1,0:T(8,128)(2,1)} %w_ref.1) | copy-start | bytes 3145732
  13.0 6.7 %copy-start.6 = (f32[2,256]{1,0:T(2,128)S(1)}, f32[2,256]{1,0:T(2,128)}, u32[]{:S(2)}) copy-start(f32[2,256]{1,0:T(2,128)} %m_ref.1) | copy-start | bytes 6148
  13.1 6.8 %copy-start.7 = (f32[128]{0:T(128)S(1)}, f32[128]{0:T(128)}, u32[]{:S(2)}) copy-start(f32[128]{0:T(128)} %param.19) | copy-start | bytes 1540
  13.1 61.7 %all-to-all-start = ((bf16[4,96,2048]{2,1,0:T(8,128)(2,1)}), bf16[4,96,2048]{2,1,0:T(8,128)(2,1)S(1)}, u32[]{:S(2)}, u32[]{:S(2)}) async-start(bf16[4,96,2048]{2,1,0:T(8,128)(2,1)} %bitcast.19), calls=%async_computation.1 | async-start | bytes 3145728 | tf_op jit(solution)/shard_map/all_to_all | solution.py:363
  19.6 194.6 %reduce-scatter.2.cloned.1.call-start = ((), (), s32[]{:S(2)}) async-start(), calls=%async_computation.3 | async-start | bytes 5242880 | tf_op jit(solution)/shard_map/reduce_scatter | solution.py:375
  19.8 1.0 copy-start.3
  20.9 1.0 copy-start.4
  21.9 1.0 copy-start.5
  72.8 1.9 copy-start
  74.8 1.6 copy-start.1
  171.0 4.9 %copy-start.9 = (f32[128,2]{0,1:T(2,128)S(1)}, f32[128,2]{0,1:T(2,128)}, u32[]{:S(2)}) copy-start(f32[128,2]{0,1:T(2,128)} %param.24) | copy-start | bytes 3076
  171.0 41.4 %all-to-all-start.1 = ((bf16[4,96,2048]{2,1,0:T(8,128)(2,1)}), bf16[4,96,2048]{2,1,0:T(8,128)(2,1)S(1)}, u32[]{:S(2)}, u32[]{:S(2)}) async-start(bf16[4,96,2048]{2,1,0:T(8,128)(2,1)} %bitcast.7), calls=%async_computation.2 | async-start | bytes 3145728 | tf_op jit(solution)/shard_map/all_to_all | solution.py:377
Sparse Core Ops, SparseCore 0:
  74.9 69.1 reduce-scatter.1

commit v2 on v1

v2 whole, which is shorter than its diff:
```python
import functools

import jax
import jax.numpy as jnp
from jax import lax
from jax.experimental import pallas as pl
from jax.experimental.pallas import tpu as pltpu
from jax.sharding import PartitionSpec as P

HEAD_CHANNELS = 128
BLK = 128
NORM_EPS = 1e-06
CLAMP_LIMIT = 7.0
SIGMOID_SCALE = 1.702
MESH = pl.DeviceIdType.MESH
F32, BF16 = jnp.float32, jnp.bfloat16
VMEM = pl.BlockSpec(memory_space=pltpu.VMEM)
ANY = pl.BlockSpec(memory_space=pl.ANY)


def clamped_unit(gate_pre, up_pre):
    gate_pre = jnp.minimum(gate_pre, CLAMP_LIMIT)
    up_pre = jnp.clip(up_pre, -CLAMP_LIMIT, CLAMP_LIMIT)
    return (up_pre + 1.0) * gate_pre * jax.nn.sigmoid(SIGMOID_SCALE * gate_pre)


def dot(a, b, ca=1, cb=0):
    return lax.dot_general(a, b, (((ca,), (cb,)), ((), ())), preferred_element_type=F32)


def fused_kernel(
    n_ep, chunks, q_ref, g_ref, v_ref, m_ref, pos_ref, gain_ref, w_ref, rows_ref, hi_ref, lo_ref,
    gate_hbm, up_hbm, down_hbm, mix_ref, moe_ref,
    q_in, inner, inc, dec, snd, got, mixed,
    wg, wu, wd, x, xc, xp, own, mid, to_c, from_c, to_d, from_d, to_p, from_p,
    ret, mix_c, mix_d, mix_r,
    load_sem, state_send, state_recv, slot_send, slot_recv, ret_send, ret_recv,
    core_send, core_recv, link_send, link_recv,
):
    tokens, width = q_ref.shape
    heads, nblk = width // HEAD_CHANNELS, tokens // BLK
    rows, features = x.shape
    capacity, n = rows // n_ep, rows // chunks
    per = n_ep // chunks
    share = tokens // 4
    me = lax.axis_index("ep")
    t = lax.axis_index("tp")
    core = t + 1 - 2 * lax.rem(t, 2)
    peer = lax.rem(t + 2, 4)
    diag = lax.rem(core + 2, 4)

    loads = [
        pltpu.make_async_copy(s, d, load_sem.at[i])
        for i, (s, d) in enumerate(((gate_hbm, wg), (up_hbm, wu), (down_hbm, wd)))
    ]
    barrier = pltpu.get_barrier_semaphore()
    for k in range(1, n_ep):
        pl.semaphore_signal(
            barrier, inc=1, device_id={"ep": lax.rem(me + k, n_ep)}, device_id_type=MESH
        )
    for other in (core, peer):
        pl.semaphore_signal(barrier, inc=1, device_id={"tp": other}, device_id_type=MESH)
    for load in loads:
        load.start()
    pl.semaphore_wait(barrier, n_ep + 1)

    def remote(src, dst, sends, recvs, index, axis, other):
        return pltpu.make_async_remote_copy(
            src_ref=src,
            dst_ref=dst,
            send_sem=sends.at[index],
            recv_sem=recvs.at[index],
            device_id={axis: other},
            device_id_type=MESH,
        )

    def slot(k):
        return pl.ds(k * capacity, capacity)

    def part(i):
        return pl.ds(i * n, n)

    def to_core(src, dst, index):
        return remote(src, dst, core_send, core_recv, index, "tp", core)

    def to_peer(src, dst, index):
        return remote(src, dst, link_send, link_recv, index, "tp", peer)

    unsent = []
    stay = pltpu.make_async_copy(rows_ref.at[slot(0)], x.at[slot(0)], load_sem.at[3])
    stay.start()
    dispatch = [None]
    for k in range(1, n_ep):
        copy = remote(
            rows_ref.at[slot(k)], x.at[slot(k)], slot_send, slot_recv, k, "ep",
            lax.rem(me + k, n_ep),
        )
        copy.start()
        dispatch.append(copy)
        unsent.append(copy)
    stay.wait()

    gather, across = [], []

    def share_chunk(i):
        for k in range(i * per, (i + 1) * per):
            if k > 0:
                dispatch[k].wait_recv()
        copy = to_peer(x.at[part(i)], xp.at[i, 0], i)
        copy.start()
        gather.append(copy)
        unsent.append(copy)
        copy = to_core(x.at[part(i)], xc.at[part(i)], i)
        copy.start()
        across.append(copy)
        unsent.append(copy)

    share_chunk(0)

    row = lax.broadcasted_iota(jnp.int32, (BLK, BLK), 0)
    col = lax.broadcasted_iota(jnp.int32, (BLK, BLK), 1)
    masks = (row >= col, row <= col)
    floor = jnp.exp(m_ref[...])

    def cols(h):
        return slice(h * HEAD_CHANNELS, (h + 1) * HEAD_CHANNELS)

    def block_rows(b):
        return pl.ds(pl.multiple_of(b * BLK, BLK), BLK)

    def local(b, carry):
        rows = block_rows(b)
        q = q_ref[rows, :].astype(F32)
        q = q * jax.nn.sigmoid(q) * HEAD_CHANNELS ** (-0.5)
        shut = jax.nn.sigmoid(-g_ref[rows, :].astype(F32))
        v = v_ref[rows, :]
        pos_rows = pos_ref[rows, :]
        pos = jnp.concatenate(
            [jnp.broadcast_to(pos_rows[:, h : h + 1], (BLK, HEAD_CHANNELS)) for h in range(heads)],
            axis=1,
        )
        scores = [None] * heads
        for d in range(2):
            key = floor[d : d + 1, :] * shut
            rate = jnp.log1p(-key) + pos
            hi = rate.astype(BF16)
            lo = (rate - hi.astype(F32)).astype(BF16)
            tri = masks[d].astype(F32).astype(BF16)
            cumul = dot(tri, hi) + dot(tri, lo)
            last = cumul[BLK - 1 :, :] if d == 0 else cumul[:1, :]
            query_in = (q * jnp.exp(cumul)).astype(BF16)
            key_in = (key * jnp.exp(-cumul)).astype(BF16)
            key_state = (key * jnp.exp(last - cumul)).astype(BF16)
            q_in[d, rows, :] = query_in
            dec[b, d : d + 1, :] = jnp.exp(last)
            for h in range(heads):
                s = dot(query_in[:, cols(h)], key_in[:, cols(h)], 1, 1)
                s = jnp.where(masks[d], s, 0.0)
                scores[h] = s if d == 0 else scores[h] + s
                inc[d, b, :, cols(h)] = dot(v[:, cols(h)], key_state[:, cols(h)], 0, 0)
        for h in range(heads):
            inner[rows, cols(h)] = dot(scores[h].astype(BF16), v[:, cols(h)])
        return carry

    half = nblk // 2
    lax.fori_loop(0, half, local, 0)
    if chunks > 1:
        share_chunk(1)
    lax.fori_loop(half, nblk, local, 0)

    for d in range(2):
        def advance(i, carry, d=d):
            state, total = carry
            b = i if d == 0 else nblk - 1 - i
            decay = dec[b, d : d + 1, :]
            return state * decay + inc[d, b], total * decay

        state, total = lax.fori_loop(
            0, nblk, advance, (jnp.zeros((HEAD_CHANNELS, width), F32), jnp.ones((1, width), F32))
        )
        snd[d, :HEAD_CHANNELS, :] = state.astype(BF16)
        snd[d, HEAD_CHANNELS:, :] = jnp.broadcast_to(total, (16, width)).astype(BF16)

    states = []
    for k in range(1, n_ep):
        copy = remote(
            snd, got.at[k], state_send, state_recv, k, "ep", lax.rem(me + k, n_ep)
        )
        copy.start()
        states.append(copy)
        unsent.append(copy)
    for i in range(2, chunks):
        share_chunk(i)

    def mlp(block, store):
        hidden = clamped_unit(dot(block, wg[...]), dot(block, wu[...])).astype(BF16)
        step = 512 if features % 512 == 0 else features
        for at in range(0, features, step):
            store(slice(at, at + step), dot(hidden, wd[:, at : at + step]))

    for load in loads:
        load.wait()

    def keep_own(at, value):
        own[:, at] = value

    mlp(x[...], keep_own)

    def keep_core(at, value):
        to_c[:, at] = value.astype(BF16)

    for copy in across:
        copy.wait_recv()
    mlp(xc[...], keep_core)
    give = to_core(to_c, from_c, chunks)
    give.start()

    for copy in states:
        copy.wait_recv()
    entering = []
    for d in range(2):
        state = jnp.zeros((HEAD_CHANNELS, width), F32)
        for k in range(n_ep - 1, 0, -1):
            at = k if d == 0 else n_ep - k
            valid = (me - k >= 0) if d == 0 else (me + k < n_ep)
            decay = got[at, d, HEAD_CHANNELS:, :].astype(F32)[:1, :]
            new = state * decay + got[at, d, :HEAD_CHANNELS, :].astype(F32)
            state = jnp.where(valid, new, state)
        entering.append(state)

    def ahead(b, state):
        rows = block_rows(b)
        low = state.astype(BF16)
        for h in range(heads):
            inner[rows, cols(h)] += dot(q_in[0, rows, cols(h)], low[:, cols(h)], 1, 1)
        return state * dec[b, 0:1, :] + inc[0, b]

    lax.fori_loop(0, nblk, ahead, entering[0])
    gain = gain_ref[...]

    def back(i, state):
        b = nblk - 1 - i
        rows = block_rows(b)
        low = state.astype(BF16)
        outs = []
        for h in range(heads):
            mix = inner[rows, cols(h)] + dot(q_in[1, rows, cols(h)], low[:, cols(h)], 1, 1)
            mean = jnp.mean(mix * mix, axis=-1, keepdims=True)
            outs.append((mix * lax.rsqrt(mean + NORM_EPS) * gain).astype(BF16))
        mixed[rows, :] = dot(jnp.concatenate(outs, axis=1), w_ref[...]).astype(BF16)
        return state * dec[b, 1:2, :] + inc[1, b]

    lax.fori_loop(0, nblk, back, entering[1])

    def rows_of(owner):
        return pl.ds(owner * share, share)

    mix_give = to_core(mixed.at[rows_of(core)], mix_c, chunks + 1)
    mix_swap = to_core(mixed.at[rows_of(diag)], mix_d, chunks + 2)
    base = chunks + 3
    forwards = []
    for i in range(chunks):
        gather[i].wait_recv()
        copy = to_core(xp.at[i, 0], xp.at[i, 1], base + i)
        copy.start()
        forwards.append(copy)
        unsent.append(copy)
    for copy in (mix_swap, mix_give):
        copy.start()
        unsent.append(copy)

    backs = []
    for i in range(chunks):
        forwards[i].wait_recv()

        def keep_pair(at, value, i=i):
            mid[:, at] = value[:n]
            to_d[i, :, at] = value[n:].astype(BF16)

        mlp(xp[i].reshape(2 * n, features), keep_pair)
        swap = to_core(to_d.at[i], from_d.at[i], base + chunks + i)
        swap.start()
        unsent.append(swap)
        swap.wait_recv()
        to_p[i] = (mid[...] + from_d[i].astype(F32)).astype(BF16)
        copy = to_peer(to_p.at[i], from_p.at[i], chunks + i)
        copy.start()
        backs.append(copy)
        unsent.append(copy)

    mix_swap.wait_recv()
    mix_d[...] = (mixed[rows_of(peer), :].astype(F32) + mix_d[...].astype(F32)).astype(BF16)
    mix_back = to_peer(mix_d, mix_r, 2 * chunks)
    mix_back.start()
    unsent.append(mix_back)

    give.wait()
    out = to_c
    returns = []
    for i in range(chunks):
        backs[i].wait_recv()
        out[part(i), :] = (
            own[part(i), :] + from_c[part(i), :].astype(F32) + from_p[i].astype(F32)
        ).astype(BF16)
        for k in range(i * per, (i + 1) * per):
            if k == 0:
                stay = pltpu.make_async_copy(out.at[slot(0)], ret.at[slot(0)], load_sem.at[3])
                stay.start()
            else:
                copy = remote(
                    out.at[slot(k)], ret.at[slot(k)], ret_send, ret_recv, k, "ep",
                    lax.rem(me + n_ep - k, n_ep),
                )
                copy.start()
                returns.append(copy)
                unsent.append(copy)

    mix_give.wait_recv()
    mix_back.wait_recv()
    mix_ref[...] = (
        mixed[rows_of(t), :].astype(F32) + mix_c[...].astype(F32) + mix_r[...].astype(F32)
    ).astype(BF16)
    stay.wait()
    for copy in returns:
        copy.wait_recv()
    step = 512 if features % 512 == 0 else features
    for at in range(0, features, step):
        block = ret[:, at : at + step]
        moe_ref[:, at : at + step] = (
            dot(hi_ref[...], block) + dot(lo_ref[...], block)
        ).astype(BF16)
    for copy in unsent:
        copy.wait_send()


def fused(n_ep, query, logits, value, margin, pos, gain, weight, send, hi, lo, gate, up, down):
    tokens, width = query.shape
    rows, features = send.shape
    hidden = gate.shape[1]
    nblk, share = tokens // BLK, tokens // 4
    chunks = 4 if n_ep % 4 == 0 else n_ep
    n = rows // chunks
    dma = pltpu.SemaphoreType.DMA

    def low(*shape):
        return pltpu.VMEM(shape, BF16)

    return pl.pallas_call(
        functools.partial(fused_kernel, n_ep, chunks),
        out_shape=(
            jax.ShapeDtypeStruct((share, features), BF16),
            jax.ShapeDtypeStruct((hi.shape[0], features), BF16),
        ),
        in_specs=[VMEM] * 10 + [ANY] * 3,
        out_specs=(VMEM, VMEM),
        scratch_shapes=[
            low(2, tokens, width),
            pltpu.VMEM((tokens, width), F32),
            pltpu.VMEM((2, nblk, HEAD_CHANNELS, width), F32),
            pltpu.VMEM((nblk, 2, width), F32),
            low(2, HEAD_CHANNELS + 16, width),
            low(n_ep, 2, HEAD_CHANNELS + 16, width),
            low(tokens, features),
            low(features, hidden),
            low(features, hidden),
            low(hidden, features),
            low(rows, features),
            low(rows, features),
            low(chunks, 2, n, features),
            pltpu.VMEM((rows, features), F32),
            pltpu.VMEM((n, features), F32),
            low(rows, features),
            low(rows, features),
            low(chunks, n, features),
            low(chunks, n, features),
            low(chunks, n, features),
            low(chunks, n, features),
            low(rows, features),
            low(share, features),
            low(share, features),
            low(share, features),
            dma((4,)),
            dma((n_ep,)),
            dma((n_ep,)),
            dma((n_ep,)),
            dma((n_ep,)),
            dma((n_ep,)),
            dma((n_ep,)),
            dma((3 * chunks + 3,)),
            dma((3 * chunks + 3,)),
            dma((2 * chunks + 1,)),
            dma((2 * chunks + 1,)),
        ],
        compiler_params=pltpu.CompilerParams(
            collective_id=0, has_side_effects=True, vmem_limit_bytes=61 << 20
        ),
        name="fused",
    )(query, logits, value, margin, pos, gain, weight, send, hi, lo, gate, up, down)


def body(
    query,
    forget_gate_logits,
    value,
    forget_lower_margin,
    position_log_decay,
    head_norm_gain,
    mixer_output_weight,
    second_batch_tokens,
    expert_norm_gain,
    routes,
    chosen_expert_weight,
    gate_weight,
    up_weight,
    down_weight,
):
    tokens, top_count = routes.shape
    features = second_batch_tokens.shape[1]
    n_ep = lax.axis_size("ep")
    capacity = (3 * tokens * top_count + 2 * n_ep - 1) // (2 * n_ep)
    capacity = -(-capacity // 16) * 16
    tokens_f = second_batch_tokens.astype(F32)
    normed = (
        tokens_f
        * lax.rsqrt(jnp.mean(tokens_f * tokens_f, axis=-1, keepdims=True) + NORM_EPS)
        * expert_norm_gain
    ).astype(BF16)
    ahead = jnp.mod(routes - lax.axis_index("ep"), n_ep)
    named = ahead[:, :, None] == jnp.arange(n_ep, dtype=jnp.int32)[None, None, :]
    chosen = jnp.any(named, axis=1)
    earlier = jnp.tril(jnp.ones((tokens, tokens), BF16), -1)
    ranking = dot(earlier, chosen.astype(BF16)).astype(jnp.int32)
    slot = jnp.where(named, ranking[:, None, :] + jnp.arange(n_ep) * capacity, 0)
    destination = jnp.sum(slot, axis=2)
    places = jnp.arange(n_ep * capacity, dtype=jnp.int32)
    hit = destination[:, :, None] == places
    pick = jnp.any(hit, axis=1).astype(BF16)
    share = jnp.sum(jnp.where(hit, chosen_expert_weight[:, :, None], 0.0), axis=1)
    share_hi = share.astype(BF16)
    share_lo = (share - share_hi.astype(F32)).astype(BF16)
    send = dot(pick, normed, 0, 0).astype(BF16)
    return fused(
        n_ep,
        query,
        forget_gate_logits,
        value,
        forget_lower_margin,
        jnp.transpose(position_log_decay),
        head_norm_gain[None, :],
        mixer_output_weight,
        send,
        share_hi,
        share_lo,
        gate_weight[0],
        up_weight[0],
        down_weight[0],
    )


def solution(mesh):
    return jax.shard_map(
        body,
        mesh=mesh,
        in_specs=(
            P(("grp", "ep"), "tp"),
            P(("grp", "ep"), "tp"),
            P(("grp", "ep"), "tp"),
            P(None, "tp"),
            P("tp", ("grp", "ep")),
            P(),
            P("tp", None),
            P(("grp", "ep", "tp"), None),
            P(),
            P(("grp", "ep", "tp"), None),
            P(("grp", "ep", "tp"), None),
            P("ep", None, "tp"),
            P("ep", None, "tp"),
            P("ep", "tp", None),
        ),
        out_specs=(P(("grp", "ep", "tp"), None), P(("grp", "ep", "tp"), None)),
        check_vma=False,
    )
```

time: 222 us -> 140 us (0.63)
  waiting for transfers between devices: 36.4 us -> 0 us
  Pallas kernels: 145 us -> 125 us
  between operations: 14.2 us -> 0.69 us
  starting transfers between devices: 11.4 us -> 0 us
    all_to_all x2 -> x0, waiting for transfers between devices: 36.4 us -> none  [the longest x1 36.4 us: body(): lax.all_to_all(expert_sum, 'ep', split_axis=0, concat_axis=0, tiled=True)]
    pallas_call x2 -> x1, Pallas kernels: 145 us -> 125 us  [fused(): pl.pallas_call(functools.partial(fused_kernel, n_ep, chunks), out_shape=(...]
    all_to_all x2 -> x0, starting transfers between devices: 11.4 us -> none  [the longest x1 6.49 us: body(): lax.all_to_all(send, 'ep', split_axis=0, concat_axis=0, tiled=True)]
    dot_general x4 -> x2, matrix products: 4.77 us -> 2.72 us  [dot(): lax.dot_general(a, b, (((ca,), (cb,)), ((), ())), preferred_element_type=...]
    unnamed x21 -> x7, local copies, waits for them, and re-layouts: 6.86 us -> 4.88 us
  transfers between devices with their start and end apart: 3 -> 0, of which waited for: 1 -> 0; matrix products, arithmetic and copies ran while one was open for 1% -> 0% of each run, Pallas kernels for 65% -> 0%
where the time goes in v2:
time: 140 us; the launch traced here: 137 us
  Pallas kernels  125 us (89%)
  local copies, waits for them, and re-layouts  4.88 us (3%)
  other arithmetic  3.67 us (3%)
  matrix products  2.72 us (2%)
    pallas_call x1, Pallas kernels, fused(): pl.pallas_call(functools.partial(fused_kernel, n_ep, chunks), out_shape=(...  125 us
    unnamed x7, local copies, waits for them, and re-layouts  4.88 us

profile of v2, /device:TPU:0, one launch (start us, length us, event | category | flops | bytes accessed | tf_op | source)
XLA Modules:
  0.0 137.3 jit_solution(326273473551585144)
XLA Ops:
  0.6 0.0 copy-start
  0.6 0.7 and_select_fusion
  1.4 1.2 fusion.1
  2.7 0.2 fusion
  2.9 0.1 fusion.7
  3.0 0.8 select_reduce_fusion
  3.9 0.7 subtract_convert_fusion
  4.6 1.7 %copy.20 = f32[2,1024]{0,1:T(8,128)} copy(f32[2,1024]{1,0:T(2,128)} %param.18) | data formatting | bytes 16384 | tf_op args[4]
  6.3 0.0 copy-done
  6.3 2.5 %convolution_convert_fusion.rows_ref = bf16[384,2048]{1,0:T(8,128)(2,1)} fusion(pred[128,384]{1,0:T(8,128)(4,1)S(1)} %fusion.7, bf16[128,2048]{1,0:T(8,128)(2,1)S(1)} %copy-done, f32[2048]{0:T(1024)} %param.22, f32[128]{0:T(128)S(1)} %add_rsqrt_fusion), kind=kOutput, calls=%fused_computation | convolution fusion | flops 203161600 | bytes 2155008 | tf_op jit(solution)/shard_map/dot_general | solution.py:28
  8.8 125.3 %fused.1 = (bf16[256,2048]{1,0:T(8,128)(2,1)}, bf16[128,2048]{1,0:T(8,128)(2,1)}) custom-call(bf16[1024,256]{1,0:T(8,128)(2,1)} %q_ref.1, bf16[1024,256]{1,0:T(8,128)(2,1)} %g_ref.1, bf16[1024,256]{1,0:T(8,128)(2,1)} %v_ref.1, f32[2,256]{1,0:T(2,128)} %m_ref.1, f32[1024,2]{1,0:T(8,128)} %bitcast.7, f32[1,128]{1,0:T(1,128)} %bitcast.11, ...), custom_call_target="tpu_custom_call" | custom-call | tf_op jit(solution)/shard_map/fused/pallas_call | solution.py:348
  134.1 0.0 copy-start.1
  134.1 2.4 %copy.23 = bf16[256,2048]{1,0:T(8,128)(2,1)} copy(bf16[256,2048]{1,0:T(8,128)(2,1)} %get-tuple-element.6) | data formatting | bytes 2097152
  136.5 0.0 copy-done.1
  136.5 0.8 copy.24
  (5 shorter events, 0.1 us)
Async XLA Ops:
  0.6 5.6 %copy-start = (bf16[128,2048]{1,0:T(8,128)(2,1)S(1)}, bf16[128,2048]{1,0:T(8,128)(2,1)}, u32[]{:S(2)}) copy-start(bf16[128,2048]{1,0:T(8,128)(2,1)} %param.21) | copy-start | bytes 1572868
  134.1 2.4 %copy-start.1 = (bf16[128,2048]{1,0:T(8,128)(2,1)S(1)}, bf16[128,2048]{1,0:T(8,128)(2,1)}, u32[]{:S(2)}) copy-start(bf16[128,2048]{1,0:T(8,128)(2,1)} %get-tuple-element.7) | copy-start | bytes 1572868

commit v3 on v2

--- a/solution.py
+++ b/solution.py
@@ -189,9 +189,6 @@
         copy.start()
         states.append(copy)
         unsent.append(copy)
-    for i in range(2, chunks):
-        share_chunk(i)
-
     def mlp(block, store):
         hidden = clamped_unit(dot(block, wg[...]), dot(block, wu[...])).astype(BF16)
         step = 512 if features % 512 == 0 else features
@@ -200,6 +197,40 @@
 
     for load in loads:
         load.wait()
+
+    base = chunks + 3
+    forwards, backs = [], []
+
+    def forward_chunk(i):
+        gather[i].wait_recv()
+        copy = to_core(xp.at[i, 0], xp.at[i, 1], base + i)
+        copy.start()
+        forwards.append(copy)
+        unsent.append(copy)
+
+    def expert_chunk(i):
+        forwards[i].wait_recv()
+
+        def keep_pair(at, value):
+            mid[:, at] = value[:n]
+            to_d[i, :, at] = value[n:].astype(BF16)
+
+        mlp(xp[i].reshape(2 * n, features), keep_pair)
+        swap = to_core(to_d.at[i], from_d.at[i], base + chunks + i)
+        swap.start()
+        unsent.append(swap)
+        swap.wait_recv()
+        to_p[i] = (mid[...] + from_d[i].astype(F32)).astype(BF16)
+        copy = to_peer(to_p.at[i], from_p.at[i], chunks + i)
+        copy.start()
+        backs.append(copy)
+        unsent.append(copy)
+
+    early = max(chunks - 2, 0)
+    for i in range(early):
+        share_chunk(i + 2)
+        forward_chunk(i)
+        expert_chunk(i)
 
     def keep_own(at, value):
         own[:, at] = value
@@ -257,36 +288,13 @@
 
     mix_give = to_core(mixed.at[rows_of(core)], mix_c, chunks + 1)
     mix_swap = to_core(mixed.at[rows_of(diag)], mix_d, chunks + 2)
-    base = chunks + 3
-    forwards = []
-    for i in range(chunks):
-        gather[i].wait_recv()
-        copy = to_core(xp.at[i, 0], xp.at[i, 1], base + i)
-        copy.start()
-        forwards.append(copy)
-        unsent.append(copy)
+    for i in range(early, chunks):
+        forward_chunk(i)
     for copy in (mix_swap, mix_give):
         copy.start()
         unsent.append(copy)
-
-    backs = []
-    for i in range(chunks):
-        forwards[i].wait_recv()
-
-        def keep_pair(at, value, i=i):
-            mid[:, at] = value[:n]
-            to_d[i, :, at] = value[n:].astype(BF16)
-
-        mlp(xp[i].reshape(2 * n, features), keep_pair)
-        swap = to_core(to_d.at[i], from_d.at[i], base + chunks + i)
-        swap.start()
-        unsent.append(swap)
-        swap.wait_recv()
-        to_p[i] = (mid[...] + from_d[i].astype(F32)).astype(BF16)
-        copy = to_peer(to_p.at[i], from_p.at[i], chunks + i)
-        copy.start()
-        backs.append(copy)
-        unsent.append(copy)
+    for i in range(early, chunks):
+        expert_chunk(i)
 
     mix_swap.wait_recv()
     mix_d[...] = (mixed[rows_of(peer), :].astype(F32) + mix_d[...].astype(F32)).astype(BF16)

time: 140 us -> 136 us (0.971)
  the two profiles are of different devices: /device:TPU:0 before, /device:TPU:25 now
where the time goes in v3:
time: 136 us; the launch traced here: 135 us
  Pallas kernels  123 us (90%)
  local copies, waits for them, and re-layouts  4.88 us (4%)
  other arithmetic  3.67 us (3%)
  matrix products  2.72 us (2%)
    pallas_call x1, Pallas kernels, fused(): pl.pallas_call(functools.partial(fused_kernel, n_ep, chunks), out_shape=(...  123 us
    unnamed x7, local copies, waits for them, and re-layouts  4.88 us

profile of v3, /device:TPU:25, one launch (start us, length us, event | category | flops | bytes accessed | tf_op | source)
XLA Modules:
  0.0 135.2 jit_solution(7683916381656069247)
XLA Ops:
  0.6 0.0 copy-start
  0.6 0.7 and_select_fusion
  1.4 1.2 fusion.1
  2.7 0.2 fusion
  2.9 0.1 fusion.7
  3.0 0.8 select_reduce_fusion
  3.9 0.7 subtract_convert_fusion
  4.6 1.7 %copy.20 = f32[2,1024]{0,1:T(8,128)} copy(f32[2,1024]{1,0:T(2,128)} %param.18) | data formatting | bytes 16384 | tf_op args[4]
  6.3 0.0 copy-done
  6.3 2.5 %convolution_convert_fusion.rows_ref = bf16[384,2048]{1,0:T(8,128)(2,1)} fusion(pred[128,384]{1,0:T(8,128)(4,1)S(1)} %fusion.7, bf16[128,2048]{1,0:T(8,128)(2,1)S(1)} %copy-done, f32[2048]{0:T(1024)} %param.22, f32[128]{0:T(128)S(1)} %add_rsqrt_fusion), kind=kOutput, calls=%fused_computation | convolution fusion | flops 203161600 | bytes 2155008 | tf_op jit(solution)/shard_map/dot_general | solution.py:28
  8.8 123.3 %fused.1 = (bf16[256,2048]{1,0:T(8,128)(2,1)}, bf16[128,2048]{1,0:T(8,128)(2,1)}) custom-call(bf16[1024,256]{1,0:T(8,128)(2,1)} %q_ref.1, bf16[1024,256]{1,0:T(8,128)(2,1)} %g_ref.1, bf16[1024,256]{1,0:T(8,128)(2,1)} %v_ref.1, f32[2,256]{1,0:T(2,128)} %m_ref.1, f32[1024,2]{1,0:T(8,128)} %bitcast.7, f32[1,128]{1,0:T(1,128)} %bitcast.11, ...), custom_call_target="tpu_custom_call" | custom-call | tf_op jit(solution)/shard_map/fused/pallas_call | solution.py:356
  132.1 0.0 copy-start.1
  132.1 2.4 %copy.23 = bf16[256,2048]{1,0:T(8,128)(2,1)} copy(bf16[256,2048]{1,0:T(8,128)(2,1)} %get-tuple-element.6) | data formatting | bytes 2097152
  134.4 0.0 copy-done.1
  134.4 0.8 copy.24
  (5 shorter events, 0.1 us)
Async XLA Ops:
  0.6 5.6 %copy-start = (bf16[128,2048]{1,0:T(8,128)(2,1)S(1)}, bf16[128,2048]{1,0:T(8,128)(2,1)}, u32[]{:S(2)}) copy-start(bf16[128,2048]{1,0:T(8,128)(2,1)} %param.21) | copy-start | bytes 1572868
  132.1 2.4 %copy-start.1 = (bf16[128,2048]{1,0:T(8,128)(2,1)S(1)}, bf16[128,2048]{1,0:T(8,128)(2,1)}, u32[]{:S(2)}) copy-start(bf16[128,2048]{1,0:T(8,128)(2,1)} %get-tuple-element.7) | copy-start | bytes 1572868
